TPU v7x, 32 devices: a whole 2x2x4 slice. The times are simulated.
32 devices in a mesh: sp: 8 (over z, y), tp: 4 (over x, core).
Axes of the slice: x: 2, y: 2, z: 4, core: 2. Of those that a mesh axis runs over, the one named last changes fastest.
Arguments:
- skip_stream_vector: bfloat16 [8192, 2048], P(('sp', 'tp')), may hold values from -6 to 6
- probe_preactivation: bfloat16 [8192, 1024], P('sp', 'tp'), may hold values from -6 to 6
- retention_preactivation: bfloat16 [8192, 1024], P('sp', 'tp'), may hold values from -4.5 to 4.5
- content_vector: bfloat16 [8192, 1024], P('sp', 'tp'), may hold values from -6 to 6
- emission_preactivation: bfloat16 [8192, 1024], P('sp', 'tp'), may hold values from -6 to 6
- retention_slack: float32 [1024], P('tp'), may hold values from 0 to 0.12
- surge_rate: float32 [8192, 1024], P('sp', 'tp'), may hold values from -1.2 to 0
- subspace_scaling_factor: float32 [1024], P('tp'), may hold values from 0.1 to 1.9
- emission_matrix: bfloat16 [1024, 2048], replicated, may hold values from -0.1875 to 0.1875
- mlp_scaling_factor: float32 [2048], replicated, may hold values from 0.1 to 1.9
- switch_matrix: bfloat16 [2048, 5632], P('sp', 'tp'), may hold values from -0.125 to 0.125
- expansion_matrix: bfloat16 [2048, 5632], P('sp', 'tp'), may hold values from -0.125 to 0.125
- contraction_matrix: bfloat16 [5632, 2048], P('tp', 'sp'), may hold values from -0.078125 to 0.078125
Outputs:
- stream_out: bfloat16 [8192, 2048], P(('sp', 'tp'))
All inputs are finite; a program needn't handle non-finite values.
Results may differ from a plain program's by a relative error of at most 0.017.
Values may be sent and summed in bfloat16 or wider, within the bound.
A program may use at most 128 MiB of HBM per device.

v0:
```python
import jax
import jax.numpy as jnp
from jax import lax
from jax.sharding import PartitionSpec as P

HEAD_DIM = 128
BLOCK = 64
EPSILON = 1e-06
TOP_PRECISION = lax.Precision.HIGHEST


def carried_in(value, axis, join, neutral):
    place = lax.axis_index(axis)
    gathered = jax.tree.map(
        lambda a, kind: lax.all_gather(a.astype(kind), axis), value, (jnp.bfloat16, jnp.bfloat16)
    )
    state = jax.tree.map(lambda a, e: jnp.zeros_like(a) + jnp.asarray(e, a.dtype), value, neutral)

    def one(turn, state):
        return join(
            state,
            jax.tree.map(
                lambda a, own: lax.dynamic_index_in_dim(a, turn, 0, False).astype(own.dtype),
                gathered,
                value,
            ),
        )

    return lax.fori_loop(0, place, one, state)


def block_step(carry, inputs):
    memory_state, offsets = carry
    query_block, input_gate_block, value_block, log_blk = inputs
    cumulative_decay = jnp.cumsum(log_blk, axis=1)
    length = log_blk.shape[1]
    carried_share = jnp.einsum(
        "eia,eax->eix",
        query_block * jnp.exp(cumulative_decay),
        memory_state,
        precision=TOP_PRECISION,
    )
    middle = cumulative_decay[:, length // 2, :][:, None, :]
    left_side = query_block * jnp.exp(cumulative_decay - middle)
    right_side = input_gate_block * jnp.exp(middle - cumulative_decay)
    causal = (jnp.arange(length)[:, None] >= jnp.arange(length)[None, :])[None, :, :]
    scores = jnp.einsum("htk,hsk->hts", left_side, right_side, precision=TOP_PRECISION)
    scores = jnp.where(causal, scores, 0.0)
    outputs = carried_share + jnp.einsum(
        "hts,hsv->htv", scores, value_block, precision=TOP_PRECISION
    )
    closing_log_decay = cumulative_decay[:, -1, :]
    updated_memory_state = jnp.exp(closing_log_decay)[:, :, None] * memory_state + jnp.einsum(
        "qnj,qnl->qjl",
        input_gate_block * jnp.exp(closing_log_decay[:, None, :] - cumulative_decay),
        value_block,
        precision=TOP_PRECISION,
    )
    return (
        (updated_memory_state, offsets + closing_log_decay),
        (outputs, cumulative_decay + offsets[:, None, :]),
    )


def split_blocks(values, heads_here):
    count = values.shape[0]
    return values.reshape(count // BLOCK, BLOCK, heads_here, HEAD_DIM).transpose(0, 2, 1, 3)


def admission_source_matrix(
    probe_preactivation, retention_preactivation, content_vector, retention_slack, surge_rate
):
    query_act = jax.nn.silu(probe_preactivation.astype(jnp.float32))
    admission_factor = retention_slack[None, :] * jax.nn.sigmoid(
        -retention_preactivation.astype(jnp.float32)
    )
    retention_logarithm = jnp.log1p(-admission_factor) + surge_rate
    return (query_act, admission_factor, content_vector.astype(jnp.float32), retention_logarithm)


def head_output(outputs, subspace_scaling_factor, emission_preactivation):
    count, heads_here = (outputs.shape[0], outputs.shape[1])
    squares = jnp.mean(outputs * outputs, axis=-1, keepdims=True)
    scaled = (
        outputs
        * lax.rsqrt(squares + EPSILON)
        * subspace_scaling_factor.reshape(heads_here, HEAD_DIM)
    )
    scaled = scaled.reshape(count, heads_here * HEAD_DIM)
    return (scaled * jax.nn.silu(emission_preactivation.astype(jnp.float32))).astype(jnp.bfloat16)


def row_norm(stream, mlp_scaling_factor):
    streamf = stream.astype(jnp.float32)
    squares = jnp.mean(streamf * streamf, axis=-1, keepdims=True)
    return (streamf * lax.rsqrt(squares + EPSILON) * mlp_scaling_factor).astype(jnp.bfloat16)


def chain(earlier, later):
    return (earlier[0] * later[0], later[0][:, :, None] * earlier[1] + later[1])


def on_device(
    skip_stream_vector,
    probe_preactivation,
    retention_preactivation,
    content_vector,
    emission_preactivation,
    retention_slack,
    surge_rate,
    subspace_scaling_factor,
    emission_matrix,
    mlp_scaling_factor,
    switch_matrix,
    expansion_matrix,
    contraction_matrix,
):
    heads_here = probe_preactivation.shape[1] // HEAD_DIM
    tok_rows = probe_preactivation.shape[0]
    arranged_sources = admission_source_matrix(
        probe_preactivation, retention_preactivation, content_vector, retention_slack, surge_rate
    )
    block_list = tuple((split_blocks(item, heads_here) for item in arranged_sources))
    start_carry = (
        jnp.zeros((heads_here, HEAD_DIM, HEAD_DIM), jnp.float32),
        jnp.zeros((heads_here, HEAD_DIM), jnp.float32),
    )
    (memory_state, offsets), (outputs, cumulative_log_decay) = lax.scan(
        block_step, start_carry, block_list
    )
    incoming_state = carried_in(
        (jnp.exp(offsets), memory_state),
        "sp",
        chain,
        (jnp.ones_like(offsets), jnp.zeros_like(memory_state)),
    )
    outputs = outputs + jnp.einsum(
        "jmxo,mos->jmxs",
        block_list[0] * jnp.exp(cumulative_log_decay),
        incoming_state[1],
        precision=TOP_PRECISION,
    )
    outputs = outputs.transpose(0, 2, 1, 3).reshape(tok_rows, heads_here, HEAD_DIM)
    mixed = head_output(outputs, subspace_scaling_factor, emission_preactivation)
    own_width = heads_here * HEAD_DIM
    own_rows = lax.dynamic_slice_in_dim(
        emission_matrix, lax.axis_index("tp") * own_width, own_width, 0
    )
    projected = lax.psum_scatter(
        jnp.dot(mixed, own_rows, preferred_element_type=jnp.float32).astype(jnp.bfloat16),
        "tp",
        scatter_dimension=0,
        tiled=True,
    ).astype(jnp.float32)
    stream = (skip_stream_vector.astype(jnp.float32) + projected).astype(jnp.bfloat16)
    normed = row_norm(stream, mlp_scaling_factor)
    all_rows = lax.all_gather(normed, "tp", axis=0, tiled=True)
    gate_proj = jnp.dot(
        all_rows,
        lax.all_gather(switch_matrix, "sp", axis=0, tiled=True),
        preferred_element_type=jnp.float32,
    )
    up_proj = jnp.dot(
        all_rows,
        lax.all_gather(expansion_matrix, "sp", axis=0, tiled=True),
        preferred_element_type=jnp.float32,
    )
    hidden = (jax.nn.silu(gate_proj) * up_proj).astype(jnp.bfloat16)
    partial_sum = jnp.dot(
        hidden,
        lax.all_gather(contraction_matrix, "sp", axis=1, tiled=True),
        preferred_element_type=jnp.float32,
    )
    summed = lax.psum_scatter(
        partial_sum.astype(jnp.bfloat16), "tp", scatter_dimension=0, tiled=True
    ).astype(jnp.float32)
    return (stream.astype(jnp.float32) + summed).astype(jnp.bfloat16)


def solution(mesh):
    in_specs = (
        P(("sp", "tp"), None),
        P("sp", "tp"),
        P("sp", "tp"),
        P("sp", "tp"),
        P("sp", "tp"),
        P("tp"),
        P("sp", "tp"),
        P("tp"),
        P(),
        P(),
        P("sp", "tp"),
        P("sp", "tp"),
        P("tp", "sp"),
    )
    out_specs = P(("sp", "tp"), None)
    return jax.shard_map(
        on_device, mesh=mesh, in_specs=in_specs, out_specs=out_specs, check_vma=False
    )
```

profile of v0, /device:TPU:0, one launch (start us, length us, event | category | flops | bytes accessed | tf_op | source)
XLA Modules:
  0.0 522.5 jit_solution(11291250167391390919)
XLA Ops:
  7.4 2.0 divide_multiply_fusion
  9.9 1.5 reshape.84
  11.4 1.3 convert_multiply_fusion.3
  13.4 2.5 reshape.90
  16.0 55.3 %while.30 = (s32[]{:T(128)}, f32[2,128,128]{2,1,0:T(8,128)S(1)}, f32[2,128]{1,0:T(2,128)S(1)}, f32[16,2,64,128]{3,2,0,1:T(8,128)}, f32[16,2,64,128]{3,2,1,0:T(8,...) while((s32[]{:T(128)}, f32[2,128,128]{2,1,0:T(8,128)S(1)}, ...), condition=%wide.region_2.3_spmd.clone, body=%wide.region_0.2_spmd.clone.sunk | while | flops 76820992 | bytes 2124949 | solution.py:128
  16.1 0.9 constant_dynamic-slice_fusion.6
  19.6 0.9 constant_dynamic-slice_fusion.6
  23.0 0.9 constant_dynamic-slice_fusion.6
  26.5 0.9 constant_dynamic-slice_fusion.6
  29.9 0.9 constant_dynamic-slice_fusion.6
  33.4 0.9 constant_dynamic-slice_fusion.6
  36.8 0.9 constant_dynamic-slice_fusion.6
  40.3 0.9 constant_dynamic-slice_fusion.6
  43.8 0.9 constant_dynamic-slice_fusion.6
  47.2 0.9 constant_dynamic-slice_fusion.6
  50.7 0.9 constant_dynamic-slice_fusion.6
  71.3 33.0 %all-gather.1 = bf16[16,128,128]{2,1,0:T(8,128)(2,1)S(1)} all-gather(bf16[2,128,128]{2,1,0:T(8,128)(2,1)S(1)} %convert_element_type.72), channel_id=3, replica_groups=mesh['sp'=8,'tp'=4] {'sp'}, dimensions={0}, use_global_device_ids=true | all-gather | bytes 589824 | tf_op jit(solution)/shard_map/all_gather | solution.py:15
  104.3 20.7 %all-gather.2 = bf16[8,2,128]{2,1,0:T(2,128)(2,1)S(1)} all-gather(bf16[1,2,128]{2,1,0:T(2,128)(2,1)S(1)} %fusion.44), channel_id=2, replica_groups=mesh['sp'=8,'tp'=4] {'sp'}, dimensions={0}, use_global_device_ids=true | all-gather | bytes 4608 | tf_op jit(solution)/shard_map/all_gather | solution.py:15
  125.1 2.8 multiply_reduce_fusion
  129.0 1.2 mul.112
  130.3 4.6 convolution_convert_fusion.1
  135.5 41.7 %reduce-scatter.3.cloned.1.call-done = bf16[256,2048]{1,0:T(8,128)(2,1)} async-done(((bf16[1024,2048]{1,0:T(8,128)(2,1)}), bf16[256,2048]{1,0:T(8,128)(2,1)}) %reduce-scatter.3.cloned.1.call-update) | async-done | bytes 1048592 | tf_op jit(solution)/shard_map/reduce_scatter | solution.py:149
  177.3 1.6 fusion.23
  178.9 2.6 fusion.25
  183.1 44.3 %all-gather.10.cloned.1.call-done = bf16[2048,1408]{1,0:T(8,128)(2,1)} async-done(((bf16[256,1408]{1,0:T(8,128)(2,1)}), bf16[2048,1408]{1,0:T(8,128)(2,1)}) %all-gather.10.cloned.1.call-update) | async-done | bytes 5767184 | tf_op jit(solution)/shard_map/all_gather | solution.py:160
  227.3 33.9 %all-gather.8.cloned.1.call-done = bf16[1024,2048]{1,0:T(8,128)(2,1)} async-done(((bf16[256,2048]{1,0:T(8,128)(2,1)}), bf16[1024,2048]{1,0:T(8,128)(2,1)}) %all-gather.8.cloned.1.call-update) | async-done | bytes 4194320 | tf_op jit(solution)/shard_map/all_gather | solution.py:157
  261.3 11.7 %fusion.49 = f32[1024,1408]{1,0:T(8,128)} fusion(bf16[1024,2048]{1,0:T(8,128)(2,1)} %all-gather.8.cloned.1.call-done, bf16[2048,1408]{1,0:T(8,128)(2,1)} %all-gather.10.cloned.1.call-done), kind=kOutput, calls=%fused_computation.85 | convolution fusion | flops 5905580032 | bytes 15728640 | tf_op jit(solution)/shard_map/dot_general | solution.py:158
  272.9 82.5 %all-gather.12.cloned.1.call-done = bf16[2048,1408]{1,0:T(8,128)(2,1)} async-done(((bf16[256,1408]{1,0:T(8,128)(2,1)}), bf16[2048,1408]{1,0:T(8,128)(2,1)}) %all-gather.12.cloned.1.call-update) | async-done | bytes 5767184 | tf_op jit(solution)/shard_map/all_gather | solution.py:165
  355.5 93.1 %all-gather.14.cloned.1.call-done = bf16[1408,2048]{1,0:T(8,128)(2,1)} async-done(((bf16[1408,256]{1,0:T(8,128)(2,1)}), bf16[1408,2048]{1,0:T(8,128)(2,1)}) %all-gather.14.cloned.1.call-update) | async-done | bytes 5767184 | tf_op jit(solution)/shard_map/all_gather | solution.py:171
  448.6 20.6 %convolution_convert_fusion = bf16[1024,2048]{1,0:T(8,128)(2,1)} fusion(bf16[1408,2048]{1,0:T(8,128)(2,1)} %all-gather.14.cloned.1.call-done, f32[1024,1408]{1,0:T(8,128)} %fusion.49, bf16[1024,2048]{1,0:T(8,128)(2,1)} %all-gather.8.cloned.1.call-done, bf16[2048,1408]{1,0:T(8,128)(2,1)} %all-gather.12.cloned.1.call-done), kind=kOutput, calls=%fused_computation.40 | convolution fusion | flops 11821907968 | bytes 25690112 | tf_op jit(solution)/shard_map/dot_general | solution.py:169
  469.2 42.9 %reduce-scatter.5.cloned.1.call-done = bf16[256,2048]{1,0:T(8,128)(2,1)} async-done(((bf16[1024,2048]{1,0:T(8,128)(2,1)}), bf16[256,2048]{1,0:T(8,128)(2,1)}) %reduce-scatter.5.cloned.1.call-update) | async-done | bytes 1048592 | tf_op jit(solution)/shard_map/reduce_scatter | solution.py:174
  512.1 2.8 fusion.26
  (218 shorter events, 48.9 us)
Async XLA Ops:
  7.4 169.9 %reduce-scatter.3.cloned.1.call-start = ((), (), s32[]{:S(2)}) async-start(), calls=%async_computation.2 | async-start | bytes 5242880 | tf_op jit(solution)/shard_map/reduce_scatter | solution.py:149
  125.0 5.2 copy-start.3
  125.0 5.2 copy-start.4
  134.9 42.4 %copy-start = (bf16[256,2048]{1,0:T(8,128)(2,1)S(1)}, bf16[256,2048]{1,0:T(8,128)(2,1)}, u32[]{:S(2)}) copy-start(bf16[256,2048]{1,0:T(8,128)(2,1)} %param.17) | copy-start | bytes 3145732
  134.9 44.0 %copy-start.2 = (f32[2048]{0:T(1024)S(1)}, f32[2048]{0:T(1024)}, u32[]{:S(2)}) copy-start(f32[2048]{0:T(1024)} %param.26) | copy-start | bytes 24580
  134.9 92.4 %all-gather.10.cloned.1.call-start = ((), (), s32[]{:S(2)}) async-start(), calls=%async_computation.4 | async-start | bytes 6488064 | tf_op jit(solution)/shard_map/all_gather | solution.py:160
  135.5 125.8 %all-gather.8.cloned.1.call-start = ((), (), s32[]{:S(2)}) async-start(), calls=%async_computation.3 | async-start | bytes 5242880 | tf_op jit(solution)/shard_map/all_gather | solution.py:157
  181.5 174.0 %all-gather.12.cloned.1.call-start = ((), (), s32[]{:S(2)}) async-start(), calls=%async_computation.5 | async-start | bytes 6488064 | tf_op jit(solution)/shard_map/all_gather | solution.py:165
  182.1 266.5 %all-gather.14.cloned.1.call-start = ((), (), s32[]{:S(2)}) async-start(), calls=%async_computation.6 | async-start | bytes 6488064 | tf_op jit(solution)/shard_map/all_gather | solution.py:171
  182.8 329.3 %reduce-scatter.5.cloned.1.call-start = ((), (), s32[]{:S(2)}) async-start(), calls=%async_computation.7 | async-start | bytes 5242880 | tf_op jit(solution)/shard_map/reduce_scatter | solution.py:174
  469.2 42.9 %copy-start.1 = (bf16[256,2048]{1,0:T(8,128)(2,1)S(1)}, bf16[256,2048]{1,0:T(8,128)(2,1)}, u32[]{:S(2)}) copy-start(bf16[256,2048]{1,0:T(8,128)(2,1)} %reduce-scatter.3.cloned.1.call-done) | copy-start | bytes 3145732
Sparse Core Ops, SparseCore 0:
  135.0 42.1 reduce-scatter.2
  469.3 42.7 reduce-scatter.4
Sparse Core Ops, SparseCore 1:
  137.6 89.7 all-gather.9
  228.8 32.4 all-gather.7
  263.3 92.1 all-gather.11
  357.5 91.0 all-gather.13
where the time goes:
time: 524 us; the launch traced here: 522 us
  waiting for transfers between devices  340 us (65%)
  matrix products  67.3 us (13%)
  blocking collectives  53.7 us (10%)
  other arithmetic  22.3 us (4%)
  local copies, waits for them, and re-layouts  22.2 us (4%)
  between operations  15.2 us (3%)
    all_gather x1, waiting for transfers between devices, on_device(): lax.all_gather(contraction_matrix, 'sp', axis=1, tiled=True)  93.1 us
    all_gather x1, waiting for transfers between devices, on_device(): lax.all_gather(expansion_matrix, 'sp', axis=0, tiled=True)  82.5 us
    all_gather x2, blocking collectives, carried_in(): lax.all_gather(a.astype(kind), axis)  53.7 us
    all_gather x1, waiting for transfers between devices, on_device(): lax.all_gather(switch_matrix, 'sp', axis=0, tiled=True)  44.3 us
    reduce_scatter x1, waiting for transfers between devices, on_device(): lax.psum_scatter(partial_sum.astype(jnp.bfloat16), 'tp', scatter_dimensio...  42.9 us
    reduce_scatter x1, waiting for transfers between devices, on_device(): lax.psum_scatter(jnp.dot(mixed, own_rows, preferred_element_type=jnp.floa...  41.7 us
    all_gather x1, waiting for transfers between devices, on_device(): all_rows = lax.all_gather(normed, 'tp', axis=0, tiled=True)  33.9 us
    dot_general x1, matrix products, on_device(): jnp.dot(hidden, lax.all_gather(contraction_matrix, 'sp', axis=1, tiled=Tr...  20.6 us
  transfers between devices with their start and end apart: 6, of which 6 were waited for; matrix products, arithmetic and copies ran while one was open for 3% of the time, Pallas kernels for 0%

commit v1 on v0

--- a/solution.py
+++ b/solution.py
@@ -7,6 +7,17 @@
 BLOCK = 64
 EPSILON = 1e-06
 TOP_PRECISION = lax.Precision.HIGHEST
+
+
+def gather_by_hops(block, axis, dim):
+    size = lax.axis_size(axis)
+    forward = [(i, (i + 1) % size) for i in range(size)]
+    shards = [block]
+    for far in range(1, size):
+        shards = [lax.ppermute(shards[0], axis, forward), *shards]
+    whole = jnp.concatenate(shards, axis=dim)
+    places = (lax.axis_index(axis) + 1) * shards[-1].shape[dim]
+    return jnp.roll(whole, places, axis=dim)
 
 
 def carried_in(value, axis, join, neutral):
@@ -154,7 +165,7 @@
     ).astype(jnp.float32)
     stream = (skip_stream_vector.astype(jnp.float32) + projected).astype(jnp.bfloat16)
     normed = row_norm(stream, mlp_scaling_factor)
-    all_rows = lax.all_gather(normed, "tp", axis=0, tiled=True)
+    all_rows = gather_by_hops(normed, "tp", 0)
     gate_proj = jnp.dot(
         all_rows,
         lax.all_gather(switch_matrix, "sp", axis=0, tiled=True),

time: 524 us -> 488 us (0.931)
  waiting for transfers between devices: 340 us -> 292 us
  local copies, waits for them, and re-layouts: 22.2 us -> 35.7 us
    all_gather x1, waiting for transfers between devices: 44.3 us -> 0.01 us  [on_device(): lax.all_gather(switch_matrix, 'sp', axis=0, tiled=True)]
    ppermute x0 -> x3, waiting for transfers between devices: none -> 43.1 us  [gather_by_hops(): shards = [lax.ppermute(shards[0], axis, forward), *shards]]
    all_gather x1 -> x0, waiting for transfers between devices: 33.9 us -> none  [on_device(): all_rows = lax.all_gather(normed, 'tp', axis=0, tiled=True)]
    all_gather x1, waiting for transfers between devices: 93.1 us -> 71.2 us  [on_device(): lax.all_gather(contraction_matrix, 'sp', axis=1, tiled=True)]
    unnamed x10 -> x17, local copies, waits for them, and re-layouts: 0.02 us -> 12.5 us
    all_gather x1, waiting for transfers between devices: 82.5 us -> 92.4 us  [on_device(): lax.all_gather(expansion_matrix, 'sp', axis=0, tiled=True)]
  transfers between devices with their start and end apart: 6 -> 8, of which waited for: 6 -> 7; matrix products, arithmetic and copies ran while one was open for 3% -> 6% of each run, Pallas kernels for 0% -> 0%
where the time goes in v1:
time: 488 us; the launch traced here: 487 us
  waiting for transfers between devices  292 us (60%)
  matrix products  67.3 us (14%)
  blocking collectives  53.8 us (11%)
  local copies, waits for them, and re-layouts  35.7 us (7%)
  other arithmetic  21.3 us (4%)
  between operations  15.2 us (3%)
    all_gather x1, waiting for transfers between devices, on_device(): lax.all_gather(expansion_matrix, 'sp', axis=0, tiled=True)  92.4 us
    all_gather x1, waiting for transfers between devices, on_device(): lax.all_gather(contraction_matrix, 'sp', axis=1, tiled=True)  71.2 us
    all_gather x2, blocking collectives, carried_in(): lax.all_gather(a.astype(kind), axis)  53.8 us
    ppermute x3, waiting for transfers between devices, gather_by_hops(): shards = [lax.ppermute(shards[0], axis, forward), *shards]  43.1 us
    reduce_scatter x1, waiting for transfers between devices, on_device(): lax.psum_scatter(partial_sum.astype(jnp.bfloat16), 'tp', scatter_dimensio...  42.9 us
    reduce_scatter x1, waiting for transfers between devices, on_device(): lax.psum_scatter(jnp.dot(mixed, own_rows, preferred_element_type=jnp.floa...  40.5 us
    dot_general x1, matrix products, on_device(): jnp.dot(hidden, lax.all_gather(contraction_matrix, 'sp', axis=1, tiled=Tr...  20.6 us
    dynamic_slice x48, local copies, waits for them, and re-layouts, on_device(): lax.scan(block_step, start_carry, block_list)  14.5 us
  transfers between devices with their start and end apart: 8, of which 7 were waited for; matrix products, arithmetic and copies ran while one was open for 6% of the time, Pallas kernels for 0%

profile of v1, /device:TPU:0, one launch (start us, length us, event | category | flops | bytes accessed | tf_op | source)
XLA Modules:
  0.0 486.5 jit_solution(2251178130423047640)
XLA Ops:
  7.4 2.0 divide_multiply_fusion
  9.9 1.5 reshape.84
  11.4 1.3 convert_multiply_fusion.3
  13.4 2.6 reshape.90
  16.0 55.3 %while.30 = (s32[]{:T(128)}, f32[2,128,128]{2,1,0:T(8,128)S(1)}, f32[2,128]{1,0:T(2,128)S(1)}, f32[16,2,64,128]{3,2,0,1:T(8,128)}, f32[16,2,64,128]{3,2,1,0:T(8,...) while((s32[]{:T(128)}, f32[2,128,128]{2,1,0:T(8,128)S(1)}, ...), condition=%wide.region_2.3_spmd.clone, body=%wide.region_0.2_spmd.clone.sunk | while | flops 76820992 | bytes 2124949 | solution.py:139
  16.1 0.9 constant_dynamic-slice_fusion.6
  19.6 0.9 constant_dynamic-slice_fusion.6
  71.3 33.2 %all-gather.1 = bf16[16,128,128]{2,1,0:T(8,128)(2,1)S(1)} all-gather(bf16[2,128,128]{2,1,0:T(8,128)(2,1)S(1)} %convert_element_type.72), channel_id=3, replica_groups=mesh['sp'=8,'tp'=4] {'sp'}, dimensions={0}, use_global_device_ids=true | all-gather | bytes 589824 | tf_op jit(solution)/shard_map/all_gather | solution.py:26
  104.5 20.7 %all-gather.2 = bf16[8,2,128]{2,1,0:T(2,128)(2,1)S(1)} all-gather(bf16[1,2,128]{2,1,0:T(2,128)(2,1)S(1)} %fusion.50), channel_id=2, replica_groups=mesh['sp'=8,'tp'=4] {'sp'}, dimensions={0}, use_global_device_ids=true | all-gather | bytes 4608 | tf_op jit(solution)/shard_map/all_gather | solution.py:26
  125.2 2.8 multiply_reduce_fusion
  129.1 1.2 mul.115
  130.3 4.6 convolution_convert_fusion.1
  136.7 40.5 %reduce-scatter.3.cloned.1.call-done = bf16[256,2048]{1,0:T(8,128)(2,1)} async-done(((bf16[1024,2048]{1,0:T(8,128)(2,1)}), bf16[256,2048]{1,0:T(8,128)(2,1)}) %reduce-scatter.3.cloned.1.call-update) | async-done | bytes 1048592 | tf_op jit(solution)/shard_map/reduce_scatter | solution.py:160
  177.3 1.6 fusion.29
  178.9 1.7 fusion.31
  180.7 14.2 %collective-permute-done = bf16[256,2048]{1,0:T(8,128)(2,1)S(1)} collective-permute-done((bf16[256,2048]{1,0:T(8,128)(2,1)S(1)}, bf16[256,2048]{1,0:T(8,128)(2,1)S(1)}, u32[]{:S(2)}, u32[]{:S(2)}) %collective-permute-start) | collective-permute-done | bytes 1048608 | tf_op jit(solution)/shard_map/ppermute | solution.py:17
  194.9 14.3 %collective-permute-done.1 = bf16[256,2048]{1,0:T(8,128)(2,1)} collective-permute-done((bf16[256,2048]{1,0:T(8,128)(2,1)S(1)}, bf16[256,2048]{1,0:T(8,128)(2,1)}, u32[]{:S(2)}, u32[]{:S(2)}) %collective-permute-start.1) | collective-permute-done | bytes 1048608 | tf_op jit(solution)/shard_map/ppermute | solution.py:17
  209.2 14.5 %collective-permute-done.2 = bf16[256,2048]{1,0:T(8,128)(2,1)} collective-permute-done((bf16[256,2048]{1,0:T(8,128)(2,1)}, bf16[256,2048]{1,0:T(8,128)(2,1)}, u32[]{:S(2)}, u32[]{:S(2)}) %collective-permute-start.2) | collective-permute-done | bytes 1048608 | tf_op jit(solution)/shard_map/ppermute | solution.py:17
  223.8 2.3 constant_dynamic-update-slice_fusion.7
  226.1 2.3 constant_dynamic-update-slice_fusion.6
  228.4 1.0 constant_dynamic-update-slice_fusion.5
  229.5 1.1 constant_dynamic-update-slice_fusion.4
  230.5 2.3 constant_dynamic-update-slice_fusion.3
  232.8 2.3 constant_dynamic-update-slice_fusion.2
  235.2 1.1 constant_dynamic-update-slice_fusion.1
  236.2 1.1 constant_dynamic-update-slice_fusion
  237.3 11.7 %fusion.25 = f32[1024,1408]{1,0:T(8,128)} fusion(bf16[2048,1408]{1,0:T(8,128)(2,1)} %all-gather.7.cloned.1.call-done, bf16[2048,2048]{1,0:T(8,128)(2,1)} %constant_dynamic-update-slice_fusion, s32[]{:T(128)S(6)} %select_n.29), kind=kOutput, calls=%fused_computation.44 | convolution fusion | flops 5905580032 | bytes 15728644 | tf_op jit(solution)/shard_map/dot_general | solution.py:169
  249.1 71.2 %all-gather.11.cloned.1.call-done = bf16[1408,2048]{1,0:T(8,128)(2,1)} async-done(((bf16[1408,256]{1,0:T(8,128)(2,1)}), bf16[1408,2048]{1,0:T(8,128)(2,1)}) %all-gather.11.cloned.1.call-update) | async-done | bytes 5767184 | tf_op jit(solution)/shard_map/all_gather | solution.py:182
  320.3 92.4 %all-gather.9.cloned.1.call-done = bf16[2048,1408]{1,0:T(8,128)(2,1)} async-done(((bf16[256,1408]{1,0:T(8,128)(2,1)}), bf16[2048,1408]{1,0:T(8,128)(2,1)}) %all-gather.9.cloned.1.call-update) | async-done | bytes 5767184 | tf_op jit(solution)/shard_map/all_gather | solution.py:176
  412.7 20.6 %convolution_convert_fusion = bf16[1024,2048]{1,0:T(8,128)(2,1)} fusion(bf16[1408,2048]{1,0:T(8,128)(2,1)} %all-gather.11.cloned.1.call-done, f32[1024,1408]{1,0:T(8,128)} %fusion.25, bf16[2048,1408]{1,0:T(8,128)(2,1)} %all-gather.9.cloned.1.call-done, bf16[2048,2048]{1,0:T(8,128)(2,1)} %constant_dynamic-update-slice_fusion, s32[]{:T(128)S(6)} %select_n.29), kind=kOutput, calls=%fused_computation.40 | convolution fusion | flops 11821907968 | bytes 25690116 | tf_op jit(solution)/shard_map/dot_general | solution.py:180
  433.4 42.9 %reduce-scatter.5.cloned.1.call-done = bf16[256,2048]{1,0:T(8,128)(2,1)} async-done(((bf16[1024,2048]{1,0:T(8,128)(2,1)}), bf16[256,2048]{1,0:T(8,128)(2,1)}) %reduce-scatter.5.cloned.1.call-update) | async-done | bytes 1048592 | tf_op jit(solution)/shard_map/reduce_scatter | solution.py:185
  476.2 2.7 fusion.32
  (229 shorter events, 56.5 us)
Async XLA Ops:
  7.4 169.9 %reduce-scatter.3.cloned.1.call-start = ((), (), s32[]{:S(2)}) async-start(), calls=%async_computation.2 | async-start | bytes 5242880 | tf_op jit(solution)/shard_map/reduce_scatter | solution.py:160
  71.3 59.0 %copy-start.3 = (bf16[1024,256]{1,0:T(8,128)(2,1)S(1)}, bf16[1024,256]{1,0:T(8,128)(2,1)}, u32[]{:S(2)}) copy-start(bf16[1024,256]{1,0:T(8,128)(2,1)} %param.21) | copy-start | bytes 1572868
  71.3 59.0 %copy-start.4 = (f32[256]{0:T(256)S(1)}, f32[256]{0:T(256)}, u32[]{:S(2)}) copy-start(f32[256]{0:T(256)} %param.24) | copy-start | bytes 3076
  134.9 42.4 %copy-start = (bf16[256,2048]{1,0:T(8,128)(2,1)S(1)}, bf16[256,2048]{1,0:T(8,128)(2,1)}, u32[]{:S(2)}) copy-start(bf16[256,2048]{1,0:T(8,128)(2,1)} %param.17) | copy-start | bytes 3145732
  134.9 44.0 %copy-start.2 = (f32[2048]{0:T(1024)S(1)}, f32[2048]{0:T(1024)}, u32[]{:S(2)}) copy-start(f32[2048]{0:T(1024)} %param.26) | copy-start | bytes 24580
  134.9 102.4 %all-gather.7.cloned.1.call-start = ((), (), s32[]{:S(2)}) async-start(), calls=%async_computation.3 | async-start | bytes 6488064 | tf_op jit(solution)/shard_map/all_gather | solution.py:171
  135.5 184.8 %all-gather.11.cloned.1.call-start = ((), (), s32[]{:S(2)}) async-start(), calls=%async_computation.5 | async-start | bytes 6488064 | tf_op jit(solution)/shard_map/all_gather | solution.py:182
  136.1 276.6 %all-gather.9.cloned.1.call-start = ((), (), s32[]{:S(2)}) async-start(), calls=%async_computation.4 | async-start | bytes 6488064 | tf_op jit(solution)/shard_map/all_gather | solution.py:176
  136.7 339.6 %reduce-scatter.5.cloned.1.call-start = ((), (), s32[]{:S(2)}) async-start(), calls=%async_computation.6 | async-start | bytes 5242880 | tf_op jit(solution)/shard_map/reduce_scatter | solution.py:185
  180.6 14.3 %collective-permute-start = (bf16[256,2048]{1,0:T(8,128)(2,1)S(1)}, bf16[256,2048]{1,0:T(8,128)(2,1)S(1)}, u32[]{:S(2)}, u32[]{:S(2)}) collective-permute-start(bf16[256,2048]{1,0:T(8,128)(2,1)S(1)} %fusion.31), channel_id=1, source_target_pairs={{0,1},{1,2},{2,3},{3,0},{4,5},{5,6},{6,7},{7,4},{8,9},{9,10},{10,1... | collective-permute-start | bytes 3145736 | tf_op jit(solution)/shard_map/ppermute | solution.py:17
  194.9 14.3 %collective-permute-start.1 = (bf16[256,2048]{1,0:T(8,128)(2,1)S(1)}, bf16[256,2048]{1,0:T(8,128)(2,1)}, u32[]{:S(2)}, u32[]{:S(2)}) collective-permute-start(bf16[256,2048]{1,0:T(8,128)(2,1)S(1)} %collective-permute-done), channel_id=1, source_target_pairs={{0,1},{1,2},{2,3},{3,0},{4,5},{5,6},{6,7},{7,4},{8,9},{9,10},{10,1... | collective-permute-start | bytes 3145736 | tf_op jit(solution)/shard_map/ppermute | solution.py:17
  209.2 14.5 %collective-permute-start.2 = (bf16[256,2048]{1,0:T(8,128)(2,1)}, bf16[256,2048]{1,0:T(8,128)(2,1)}, u32[]{:S(2)}, u32[]{:S(2)}) collective-permute-start(bf16[256,2048]{1,0:T(8,128)(2,1)} %collective-permute-done.1), channel_id=1, source_target_pairs={{0,1},{1,2},{2,3},{3,0},{4,5},{5,6},{6,7},{7,4},{8,9},{9,10},{10,1... | collective-permute-start | bytes 3145736 | tf_op jit(solution)/shard_map/ppermute | solution.py:17
  249.1 227.2 %copy-start.1 = (bf16[256,2048]{1,0:T(8,128)(2,1)S(1)}, bf16[256,2048]{1,0:T(8,128)(2,1)}, u32[]{:S(2)}) copy-start(bf16[256,2048]{1,0:T(8,128)(2,1)} %reduce-scatter.3.cloned.1.call-done) | copy-start | bytes 3145732
Sparse Core Ops, SparseCore 0:
  135.0 42.1 reduce-scatter.2
  433.5 42.7 reduce-scatter.4
Sparse Core Ops, SparseCore 1:
  137.6 89.7 all-gather.6
  229.3 91.0 all-gather.10
  322.4 90.3 all-gather.8
